TPU v7x, 512 devices: a whole 4x4x16 slice. The times are simulated.
512 devices in a mesh: ep: 32 (over z, core), tp: 16 (over y, x).
Axes of the slice: x: 4, y: 4, z: 16, core: 2. Of those that a mesh axis runs over, the one named last changes fastest.
Arguments:
- outer_gate: bfloat16 [4096, 2048], P('ep', 'tp'), may hold values from -6 to 6
- inner_gate: bfloat16 [4096, 2048], P('ep', 'tp'), may hold values from -6 to 6
- conv_value: bfloat16 [4096, 2048], P('ep', 'tp'), may hold values from -6 to 6
- conv_taps: bfloat16 [3, 2048], P(None, 'tp'), may hold values from -3.5 to 3.5
- mix_out: bfloat16 [2048, 2048], P(None, 'tp')
- gain_mixer: bfloat16 [2048], P('tp'), may hold values from 0.099609375 to 1.8984375
- bias_mixer: bfloat16 [2048], P('tp'), may hold values from -3 to 3
- moe_input: bfloat16 [4096, 2048], P('ep'), may hold values from -6 to 6
- route_ids: int32 [4096, 4], P('ep'), may hold values from 0 to 31, all different within a row; in each aligned block of 128 rows (0 to 127, 128 to 255, ...) at most 24 rows name the same one
- route_weights: float32 [4096, 4], P('ep'), may hold values from 0.1 to 1.2
- expert_gate: bfloat16 [32, 2048, 2048], P('ep', None, 'tp'), may hold values from -0.125 to 0.125
- expert_up: bfloat16 [32, 2048, 2048], P('ep', None, 'tp'), may hold values from -0.125 to 0.125
- expert_down: bfloat16 [32, 2048, 2048], P('ep', None, 'tp')
- shared_gate: bfloat16 [2048, 2048], P(None, 'tp'), may hold values from -0.125 to 0.125
- shared_up: bfloat16 [2048, 2048], P(None, 'tp'), may hold values from -0.125 to 0.125
- shared_down: bfloat16 [2048, 2048], P(None, 'tp')
- gain_experts: bfloat16 [2048], P('tp'), may hold values from 0.099609375 to 1.8984375
- bias_experts: bfloat16 [2048], P('tp'), may hold values from -3 to 3
Outputs:
- out_mixer: bfloat16 [4096, 2048], P('ep', 'tp')
- out_experts: bfloat16 [4096, 2048], P('ep', 'tp')
Inputs may be any that keep to these rules, and one draw needn't show every extreme that they name: `route_ids`: each row names 4 different experts. Among the rows of one index of ep (aligned blocks of 128 rows) no expert is named more than 24 times, a bound that some block reaches.
All inputs are finite; a program needn't handle non-finite values.
Results may differ from a plain program's by a relative error of at most 0.0055.
Values may be sent and summed in bfloat16 or wider, within the bound.
No kernel may reach another device: no remote copies, remote signals or barrier semaphores. Data moves between devices by JAX's collectives and lax.ppermute only.
A program may use at most 64 MiB of HBM per device.

v0:
```python
import jax
import jax.numpy as jnp
from jax import lax
from jax.sharding import Mesh
from jax.sharding import PartitionSpec as P

SEQS = 1
TP = ("tp_0", "tp_1")


def shifted(block, axis, distance):
    devices = range(lax.axis_size(axis))
    route = [(i - distance, i) for i in devices if i - distance in devices]
    return lax.ppermute(block, axis, route)


def from_everyone(x, axis):
    copies = jnp.broadcast_to(x, (lax.axis_size(axis), *x.shape))
    return lax.all_to_all(copies, axis, split_axis=0, concat_axis=0, tiled=True)


def laid_out(parts, dim):
    dims = list(parts.shape[1:])
    dims[dim] *= parts.shape[0]
    return jnp.moveaxis(parts, 0, dim).reshape(dims)


def gather_directly(x, axis, dim):
    parts = from_everyone(x, axis)
    return laid_out(parts, dim)


def whole_of(x, axes, dim):
    out = x
    for number in range(len(axes) - 1, -1, -1):
        out = lax.all_gather(out, axes[number], axis=dim, tiled=True)
    return out


def over_copies(x, axis):
    return from_everyone(x, axis).sum(axis=0)


def packed_total(arrays, axis):
    ends = [0]
    for a in arrays:
        ends.append(ends[-1] + a.size)
    so_far = over_copies(jnp.concatenate([a.ravel() for a in arrays]), axis)
    return tuple((so_far[b:e].reshape(a.shape) for a, b, e in zip(arrays, ends, ends[1:])))


def finish(values, totals, squares, full_width, gain, offset_bias):
    average = (totals / full_width)[:, None]
    spread = (squares / full_width)[:, None] - average * average
    scaled = (values - average) * lax.rsqrt(spread + 1e-05)
    return (scaled * gain.astype(jnp.float32) + offset_bias.astype(jnp.float32)).astype(
        jnp.bfloat16
    )


def on_device(
    outer_gate,
    inner_gate,
    conv_value,
    conv_taps,
    mix_out,
    gain_mixer,
    bias_mixer,
    moe_input,
    route_ids,
    route_weights,
    expert_gate,
    expert_up,
    expert_down,
    shared_gate,
    shared_up,
    shared_down,
    gain_experts,
    bias_experts,
):
    token_rows = outer_gate.shape[0]
    column_count = outer_gate.shape[1]
    ep_count = lax.axis_size("ep")
    tp_count = lax.axis_size(TP)
    taps_count = conv_taps.shape[0]
    product = (inner_gate.astype(jnp.float32) * conv_value.astype(jnp.float32)).astype(jnp.bfloat16)
    border = shifted(product[token_rows - (taps_count - 1) :], "ep", 1)
    extended = jnp.concatenate([border, product], axis=0).astype(jnp.float32)
    seq_length = token_rows * ep_count // SEQS
    places = (
        lax.axis_index("ep") * token_rows + jnp.arange(token_rows, dtype=jnp.int32)
    ) % seq_length
    convolved = jnp.zeros((token_rows, column_count), jnp.float32)
    for offset in range(taps_count):
        delay_rows = taps_count - 1 - offset
        delayed = extended[offset : offset + token_rows]
        kept_mask = (places >= delay_rows).astype(jnp.float32)[:, None]
        convolved = convolved + conv_taps[offset].astype(jnp.float32)[None, :] * delayed * kept_mask
    weighted_in = (outer_gate.astype(jnp.float32) * convolved).astype(jnp.bfloat16)
    block = mix_out
    mixed = jnp.dot(gather_directly(weighted_in, TP, 1), block, preferred_element_type=jnp.float32)
    topk_count = route_ids.shape[1]
    local_experts = expert_gate.shape[0]
    expert_count = local_experts * ep_count
    capacity = max(2, 3 * token_rows * topk_count // (2 * expert_count))
    flat_ids = route_ids.reshape(-1)
    marks = (flat_ids[:, None] == jnp.arange(expert_count, dtype=jnp.int32)[None, :]).astype(
        jnp.int32
    )
    ranks = jnp.sum((jnp.cumsum(marks, axis=0) - marks) * marks, axis=1)
    targets = flat_ids * capacity + ranks
    sources = jnp.arange(flat_ids.shape[0], dtype=jnp.int32) // topk_count
    sent_rows = lax.dynamic_slice_in_dim(
        moe_input, lax.axis_index(TP) * column_count, column_count, 1
    )
    buffer_rows = jnp.zeros((expert_count * capacity, sent_rows.shape[1]), jnp.bfloat16)
    buffer_rows = buffer_rows.at[targets].set(sent_rows[sources])
    sectioned = buffer_rows.reshape(ep_count, local_experts * capacity, sent_rows.shape[1])
    arrived = lax.all_to_all(sectioned, "ep", split_axis=0, concat_axis=0, tiled=True)
    arrived = whole_of(arrived, TP, 2)
    expert_rows = arrived.reshape(ep_count, local_experts, capacity, arrived.shape[2])
    gate_value = jnp.einsum(
        "secd,edf->secf", expert_rows, expert_gate, preferred_element_type=jnp.float32
    )
    up_value = jnp.einsum(
        "secd,edf->secf", expert_rows, expert_up, preferred_element_type=jnp.float32
    )
    hidden = (jax.nn.silu(gate_value) * up_value).astype(jnp.bfloat16)
    flat_hidden = hidden.reshape(expert_count * capacity, hidden.shape[3])
    shared_gate_value = jnp.dot(moe_input, shared_gate, preferred_element_type=jnp.float32)
    shared_up_value = jnp.dot(moe_input, shared_up, preferred_element_type=jnp.float32)
    shared_hidden = (jax.nn.silu(shared_gate_value) * shared_up_value).astype(jnp.bfloat16)
    piece = lax.all_gather(flat_hidden, TP, axis=1, tiled=True)
    block = expert_down
    shaped = piece.reshape(ep_count, local_experts, capacity, piece.shape[1])
    routed_sum = jnp.einsum("secf,efd->secd", shaped, block, preferred_element_type=jnp.float32)
    block = shared_down
    shared_sum = jnp.dot(
        gather_directly(shared_hidden, TP, 1), block, preferred_element_type=jnp.float32
    )
    expert_out = routed_sum.astype(jnp.bfloat16).reshape(
        ep_count, local_experts * capacity, column_count
    )
    returned = lax.all_to_all(expert_out, "ep", split_axis=0, concat_axis=0, tiled=True)
    picked = returned.reshape(expert_count * capacity, column_count)[targets].astype(jnp.float32)
    weighted = picked.reshape(token_rows, topk_count, column_count) * route_weights[:, :, None]
    combined = jnp.sum(weighted, axis=1) + shared_sum
    mixer_total, mixer_square, expert_total, expert_square = packed_total(
        (
            jnp.sum(mixed, axis=1),
            jnp.sum(mixed * mixed, axis=1),
            jnp.sum(combined, axis=1),
            jnp.sum(combined * combined, axis=1),
        ),
        TP,
    )
    full_width = column_count * tp_count
    out_mixer = finish(mixed, mixer_total, mixer_square, full_width, gain_mixer, bias_mixer)
    out_experts = finish(
        combined, expert_total, expert_square, full_width, gain_experts, bias_experts
    )
    return (out_mixer, out_experts)


def solution(mesh):
    split = Mesh(mesh.devices.reshape(mesh.shape["ep"], 4, 4), ("ep", "tp_0", "tp_1"))
    placed = (
        P("ep", TP),
        P("ep", TP),
        P("ep", TP),
        P(None, TP),
        P(None, TP),
        P(TP),
        P(TP),
        P("ep", None),
        P("ep", None),
        P("ep", None),
        P("ep", None, TP),
        P("ep", None, TP),
        P("ep", None, TP),
        P(None, TP),
        P(None, TP),
        P(None, TP),
        P(TP),
        P(TP),
    )
    return jax.shard_map(
        on_device,
        mesh=split,
        in_specs=placed,
        out_specs=(P("ep", TP), P("ep", TP)),
        check_vma=False,
    )
```

profile of v0, /device:TPU:2, one launch (start us, length us, event | category | flops | bytes accessed | tf_op | source)
XLA Modules:
  0.0 250.5 jit_solution(1599783190287203678)
XLA Ops:
  7.2 0.8 copy.54
  9.0 1.2 reduce-window.6
  10.7 0.8 constant_dynamic-slice_fusion
  11.6 3.0 %scatter_custom_fusion = bf16[768,128]{1,0:T(8,128)(2,1)S(1)} fusion(s32[512]{0:T(512)S(1)} %bitcast.88, bf16[128,128]{1,0:T(8,128)(2,1)S(1)} %constant_dynamic-slice_fusion, s32[1024]{0:T(1024)S(1)} %pad_clamp_fusion.1, bf16[]{:T(256)} %constant.69.clone.1), kind=kCustom, calls=%fused_computation.16 | custom fusion | bytes 196610 | tf_op jit(solution)/shard_map/scatter | solution.py:117
  14.6 35.4 %all_to_all.26 = bf16[32,24,128]{2,1,0:T(8,128)(2,1)S(1)} all-to-all(bf16[32,24,128]{2,1,0:T(8,128)(2,1)S(1)} %bitcast.85), channel_id=1, replica_groups=mesh['ep'=32,'tp_0'=4,'tp_1'=4] {'ep'}, dimensions={0} | all-to-all | bytes 393216 | tf_op jit(solution)/shard_map/all_to_all | solution.py:119
  50.0 17.1 %all_gather.9 = bf16[32,24,512]{2,1,0:T(8,128)(2,1)} all-gather(bf16[32,24,128]{2,1,0:T(8,128)(2,1)S(1)} %all_to_all.26), channel_id=1, replica_groups=mesh['ep'=32,'tp_0'=4,'tp_1'=4] {'tp_1'}, dimensions={2}, use_global_device_ids=true | all-gather | bytes 983040 | tf_op jit(solution)/shard_map/all_gather | solution.py:36
  67.2 38.3 %all-gather.3.cloned.1.call-done = bf16[32,24,2048]{2,1,0:T(8,128)(2,1)} async-done(((bf16[32,24,512]{2,1,0:T(8,128)(2,1)}), bf16[32,24,2048]{2,1,0:T(8,128)(2,1)}) %all-gather.3.cloned.1.call-update) | async-done | bytes 3145744 | tf_op jit(solution)/shard_map/all_gather | solution.py:36
  105.5 3.0 %convolution_bitcast_fusion.1 = f32[32,1,24,128]{3,2,0,1:T(8,128)S(1)} fusion(bf16[32,24,2048]{2,1,0:T(8,128)(2,1)} %all-gather.3.cloned.1.call-done, bf16[1,2048,128]{2,1,0:T(8,128)(2,1)S(1)} %copy-done), kind=kOutput, calls=%fused_computation.4 | convolution fusion | flops 402653184 | bytes 4063232 | tf_op jit(solution)/shard_map/secd,edf->secf/dot_general | solution.py:122
  108.6 1.7 fusion.1
  110.3 1.6 collective-permute-start
  112.0 0.7 collective-permute-done
  113.0 0.9 broadcast_in_dim.8
  113.9 6.2 %all-to-all-start = ((bf16[16,128,128]{1,2,0:T(8,128)(2,1)}), bf16[16,128,128]{1,2,0:T(8,128)(2,1)S(1)}, u32[]{:S(2)}, u32[]{:S(2)}) async-start(bf16[16,128,128]{1,2,0:T(8,128)(2,1)} %broadcast_in_dim.8), calls=%async_computation | async-start | bytes 1048576 | tf_op jit(solution)/shard_map/all_to_all | solution.py:19
  120.1 57.4 %all-gather.5.cloned.1.call-done = bf16[768,2048]{1,0:T(8,128)(2,1)} async-done(((bf16[768,128]{1,0:T(8,128)(2,1)}), bf16[768,2048]{1,0:T(8,128)(2,1)}) %all-gather.5.cloned.1.call-update) | async-done | bytes 3145744 | tf_op jit(solution)/shard_map/all_gather | solution.py:133
  177.5 3.6 %convolution_convert_fusion = bf16[32,24,128]{2,1,0:T(8,128)(2,1)} fusion(bf16[32,24,2048]{2,1,0:T(8,128)(2,1)} %bitcast.92, bf16[1,2048,128]{2,1,0:T(8,128)(2,1)} %param.30), kind=kOutput, calls=%fused_computation.7 | convolution fusion | flops 402751488 | bytes 3866624 | tf_op jit(solution)/shard_map/secf,efd->secd/dot_general | solution.py:136
  181.2 12.7 %all-to-all-start.2 = ((bf16[32,24,128]{2,1,0:T(8,128)(2,1)}), bf16[32,24,128]{2,1,0:T(8,128)(2,1)S(1)}, u32[]{:S(2)}, u32[]{:S(2)}) async-start(bf16[32,24,128]{2,1,0:T(8,128)(2,1)} %convolution_convert_fusion), calls=%async_computation.2 | async-start | bytes 393216 | tf_op jit(solution)/shard_map/all_to_all | solution.py:144
  194.4 1.3 fusion.2
  195.8 18.0 %all-to-all-done.2 = bf16[32,24,128]{2,1,0:T(8,128)(2,1)S(1)} async-done(((bf16[32,24,128]{2,1,0:T(8,128)(2,1)}), bf16[32,24,128]{2,1,0:T(8,128)(2,1)S(1)}, u32[]{:S(2)}, u32[]{:S(2)}) %all-to-all-start.2) | async-done | bytes 196640 | tf_op jit(solution)/shard_map/all_to_all | solution.py:144
  213.9 0.9 broadcast_in_dim.10
  214.8 5.7 %all-to-all-start.3 = ((bf16[16,128,128]{1,2,0:T(8,128)(2,1)}), bf16[16,128,128]{1,2,0:T(8,128)(2,1)S(1)}, u32[]{:S(2)}, u32[]{:S(2)}) async-start(bf16[16,128,128]{1,2,0:T(8,128)(2,1)} %broadcast_in_dim.10), calls=%async_computation.3 | async-start | bytes 1048576 | tf_op jit(solution)/shard_map/all_to_all | solution.py:19
  220.9 1.3 gather_fusion
  222.5 7.4 %all-to-all-done.3 = bf16[16,128,128]{1,2,0:T(8,128)(2,1)S(1)} async-done(((bf16[16,128,128]{1,2,0:T(8,128)(2,1)}), bf16[16,128,128]{1,2,0:T(8,128)(2,1)S(1)}, u32[]{:S(2)}, u32[]{:S(2)}) %all-to-all-start.3) | async-done | bytes 524320 | tf_op jit(solution)/shard_map/all_to_all | solution.py:19
  230.9 4.7 %all-to-all-start.4 = ((f32[16,1,512]{2,1,0:T(1,128)}), f32[16,1,512]{2,1,0:T(1,128)S(1)}, u32[]{:S(2)}, u32[]{:S(2)}) async-start(f32[16,1,512]{2,1,0:T(1,128)} %broadcast_in_dim.11), calls=%async_computation.4 | async-start | bytes 65536 | tf_op jit(solution)/shard_map/all_to_all | solution.py:19
  235.7 6.2 %all-to-all-done.4 = f32[16,1,512]{2,1,0:T(1,128)S(1)} async-done(((f32[16,1,512]{2,1,0:T(1,128)}), f32[16,1,512]{2,1,0:T(1,128)S(1)}, u32[]{:S(2)}, u32[]{:S(2)}) %all-to-all-start.4) | async-done | bytes 32800 | tf_op jit(solution)/shard_map/all_to_all | solution.py:19
  (78 shorter events, 5.9 us)
Async XLA Ops:
  7.2 98.3 %copy-start = (bf16[1,2048,128]{2,1,0:T(8,128)(2,1)S(1)}, bf16[1,2048,128]{2,1,0:T(8,128)(2,1)}, u32[]{:S(2)}) copy-start(bf16[1,2048,128]{2,1,0:T(8,128)(2,1)} %param.28) | copy-start | bytes 1572868
  7.2 98.3 %all-gather.3.cloned.1.call-start = ((), (), s32[]{:S(2)}) async-start(), calls=%async_computation.5 | async-start | bytes 3932160 | tf_op jit(solution)/shard_map/all_gather | solution.py:36
  14.6 93.9 %copy-start.11 = (bf16[1,2048,128]{2,1,0:T(8,128)(2,1)S(1)}, bf16[1,2048,128]{2,1,0:T(8,128)(2,1)}, u32[]{:S(2)}) copy-start(bf16[1,2048,128]{2,1,0:T(8,128)(2,1)} %param.29) | copy-start | bytes 1572868
  67.1 110.4 %all-gather.5.cloned.1.call-start = ((), (), s32[]{:S(2)}) async-start(), calls=%async_computation.6 | async-start | bytes 3342336 | tf_op jit(solution)/shard_map/all_gather | solution.py:133
  105.5 3.0 %copy-start.1 = (bf16[32,24,2048]{2,1,0:T(8,128)(2,1)S(1)}, bf16[32,24,2048]{2,1,0:T(8,128)(2,1)}, u32[]{:S(2)}) copy-start(bf16[32,24,2048]{2,1,0:T(8,128)(2,1)} %all-gather.3.cloned.1.call-done) | copy-start | bytes 9437188
  108.5 1.7 copy-start.6
  108.6 1.7 copy-start.7
  108.6 3.4 %copy-start.9 = (bf16[3,128]{1,0:T(4,128)(2,1)S(1)}, bf16[3,128]{1,0:T(4,128)(2,1)}, u32[]{:S(2)}) copy-start(bf16[3,128]{1,0:T(4,128)(2,1)} %param.21) | copy-start | bytes 2308
  108.6 4.2 %copy-start.8 = (bf16[128,128]{1,0:T(8,128)(2,1)S(1)}, bf16[128,128]{1,0:T(8,128)(2,1)}, u32[]{:S(2)}) copy-start(bf16[128,128]{1,0:T(8,128)(2,1)} %param.18) | copy-start | bytes 98308
  110.3 2.4 collective-permute-start
  112.7 81.1 %copy-start.10 = (f32[128,4]{0,1:T(4,128)S(1)}, f32[128,4]{0,1:T(4,128)}, u32[]{:S(2)}) copy-start(f32[128,4]{0,1:T(4,128)} %param.27) | copy-start | bytes 6148
  112.8 81.2 %copy-start.2 = (bf16[128,2048]{1,0:T(8,128)(2,1)S(1)}, bf16[128,2048]{1,0:T(8,128)(2,1)}, u32[]{:S(2)}) copy-start(bf16[128,2048]{1,0:T(8,128)(2,1)} %param.25) | copy-start | bytes 1572868
  112.8 81.2 %copy-start.4 = (bf16[2048,128]{1,0:T(8,128)(2,1)S(1)}, bf16[2048,128]{1,0:T(8,128)(2,1)}, u32[]{:S(2)}) copy-start(bf16[2048,128]{1,0:T(8,128)(2,1)} %param.31) | copy-start | bytes 1572868
  113.9 67.2 %all-to-all-start = ((bf16[16,128,128]{1,2,0:T(8,128)(2,1)}), bf16[16,128,128]{1,2,0:T(8,128)(2,1)S(1)}, u32[]{:S(2)}, u32[]{:S(2)}) async-start(bf16[16,128,128]{1,2,0:T(8,128)(2,1)} %broadcast_in_dim.8), calls=%async_computation | async-start | bytes 1048576 | tf_op jit(solution)/shard_map/all_to_all | solution.py:19
  181.2 39.3 %copy-start.3 = (bf16[2048,128]{1,0:T(8,128)(2,1)S(1)}, bf16[2048,128]{1,0:T(8,128)(2,1)}, u32[]{:S(2)}) copy-start(bf16[2048,128]{1,0:T(8,128)(2,1)} %param.22) | copy-start | bytes 1572868
  181.2 32.7 %all-to-all-start.2 = ((bf16[32,24,128]{2,1,0:T(8,128)(2,1)}), bf16[32,24,128]{2,1,0:T(8,128)(2,1)S(1)}, u32[]{:S(2)}, u32[]{:S(2)}) async-start(bf16[32,24,128]{2,1,0:T(8,128)(2,1)} %convolution_convert_fusion), calls=%async_computation.2 | async-start | bytes 393216 | tf_op jit(solution)/shard_map/all_to_all | solution.py:144
  194.0 35.9 %copy-start.5 = (bf16[2048,128]{1,0:T(8,128)(2,1)S(1)}, bf16[2048,128]{1,0:T(8,128)(2,1)}, u32[]{:S(2)}) copy-start(bf16[2048,128]{1,0:T(8,128)(2,1)} %param.33) | copy-start | bytes 1572868
  194.3 41.3 %copy-start.12 = (bf16[128]{0:T(256)(128)(2,1)S(1)}, bf16[128]{0:T(256)(128)(2,1)}, u32[]{:S(2)}) copy-start(bf16[128]{0:T(256)(128)(2,1)} %param.34) | copy-start | bytes 772
  194.3 41.3 %copy-start.13 = (bf16[128]{0:T(256)(128)(2,1)S(1)}, bf16[128]{0:T(256)(128)(2,1)}, u32[]{:S(2)}) copy-start(bf16[128]{0:T(256)(128)(2,1)} %param.35) | copy-start | bytes 772
  194.3 41.3 %copy-start.14 = (bf16[128]{0:T(256)(128)(2,1)S(1)}, bf16[128]{0:T(256)(128)(2,1)}, u32[]{:S(2)}) copy-start(bf16[128]{0:T(256)(128)(2,1)} %param.23) | copy-start | bytes 772
  194.4 41.3 %copy-start.15 = (bf16[128]{0:T(256)(128)(2,1)S(1)}, bf16[128]{0:T(256)(128)(2,1)}, u32[]{:S(2)}) copy-start(bf16[128]{0:T(256)(128)(2,1)} %param.24) | copy-start | bytes 772
  214.8 15.1 %all-to-all-start.3 = ((bf16[16,128,128]{1,2,0:T(8,128)(2,1)}), bf16[16,128,128]{1,2,0:T(8,128)(2,1)S(1)}, u32[]{:S(2)}, u32[]{:S(2)}) async-start(bf16[16,128,128]{1,2,0:T(8,128)(2,1)} %broadcast_in_dim.10), calls=%async_computation.3 | async-start | bytes 1048576 | tf_op jit(solution)/shard_map/all_to_all | solution.py:19
  230.9 11.0 %all-to-all-start.4 = ((f32[16,1,512]{2,1,0:T(1,128)}), f32[16,1,512]{2,1,0:T(1,128)S(1)}, u32[]{:S(2)}, u32[]{:S(2)}) async-start(f32[16,1,512]{2,1,0:T(1,128)} %broadcast_in_dim.11), calls=%async_computation.4 | async-start | bytes 65536 | tf_op jit(solution)/shard_map/all_to_all | solution.py:19
Sparse Core Ops, SparseCore 0:
  67.2 38.2 all-gather.2
  110.4 67.0 all-gather.4
where the time goes:
time: 251 us; the launch traced here: 250 us
  waiting for transfers between devices  128 us (51%)
  blocking collectives  52.5 us (21%)
  starting transfers between devices  30.9 us (12%)
  between operations  14.5 us (6%)
  local copies, waits for them, and re-layouts  11.1 us (4%)
  matrix products  10.7 us (4%)
  other arithmetic  2.72 us (1%)
    all_gather x1, waiting for transfers between devices, on_device(): piece = lax.all_gather(flat_hidden, TP, axis=1, tiled=True)  57.4 us
    all_gather x1, waiting for transfers between devices, whole_of(): out = lax.all_gather(out, axes[number], axis=dim, tiled=True)  38.3 us
    all_to_all x1, blocking collectives, on_device(): lax.all_to_all(sectioned, 'ep', split_axis=0, concat_axis=0, tiled=True)  35.4 us
    all_to_all x1, waiting for transfers between devices, on_device(): lax.all_to_all(expert_out, 'ep', split_axis=0, concat_axis=0, tiled=True)  18 us
    all_gather x1, blocking collectives, whole_of(): out = lax.all_gather(out, axes[number], axis=dim, tiled=True)  17.1 us
    all_to_all x3, starting transfers between devices, from_everyone(): return lax.all_to_all(copies, axis, split_axis=0, concat_axis=0, tiled=True)  16.6 us
    all_to_all x3, waiting for transfers between devices, from_everyone(): return lax.all_to_all(copies, axis, split_axis=0, concat_axis=0, tiled=True)  13.6 us
    all_to_all x1, starting transfers between devices, on_device(): lax.all_to_all(expert_out, 'ep', split_axis=0, concat_axis=0, tiled=True)  12.7 us
  transfers between devices with their start and end apart: 7, of which 6 were waited for; matrix products, arithmetic and copies ran while one was open for 3% of the time, Pallas kernels for 0%

commit v1 on v0

v1 whole, which is shorter than its diff:
```python
import jax
import jax.numpy as jnp
from jax import lax
from jax.experimental import pallas as pl
from jax.experimental.pallas import tpu as pltpu
from jax.sharding import Mesh
from jax.sharding import PartitionSpec as P

SEQS = 1
F32 = jnp.float32
BF16 = jnp.bfloat16
TP = ("y", "x")


def shifted(block, axis, distance):
    devices = range(lax.axis_size(axis))
    route = [(i - distance, i) for i in devices if i - distance in devices]
    return lax.ppermute(block, axis, route)


def exchanged(x, axis):
    return lax.all_to_all(x, axis, split_axis=0, concat_axis=0, tiled=True)


def from_everyone(x, axis):
    return exchanged(jnp.broadcast_to(x, (lax.axis_size(axis), *x.shape)), axis)


def vmem(count):
    return [pl.BlockSpec(memory_space=pltpu.VMEM) for _ in range(count)]


def iota(shape, dim):
    return lax.broadcasted_iota(jnp.int32, shape, dim)


def ordinals(ids):
    rows = ids.shape[0]
    experts = iota((rows, 128), 1)
    named = jnp.zeros((rows, 128), F32)
    for k in range(ids.shape[1]):
        named = named + (ids[:, k : k + 1] == experts).astype(F32)
    before = (iota((rows, rows), 1) <= iota((rows, rows), 0)).astype(BF16)
    place = jnp.dot(before, named.astype(BF16), preferred_element_type=F32)
    return (named * place).astype(BF16), experts


def pack_kernel(where, ids_ref, x_ref, out_ref):
    slots, blocks = 6, 4
    rows = out_ref.shape[0]
    code, _ = ordinals(ids_ref[...])
    expert_of = (iota((rows, 128), 0) // (slots * blocks) == iota((rows, 128), 1)).astype(BF16)
    spread = lax.dot_general(
        expert_of, code, (((1,), (1,)), ((), ())), preferred_element_type=F32
    )
    row = iota(spread.shape, 0)
    wanted = (row % (slots * blocks)) // blocks + (where[0] * slots + 1)
    pick = (spread == wanted.astype(F32)).astype(BF16)
    taken = jnp.dot(pick, x_ref[...], preferred_element_type=F32)
    part = iota((rows, 128), 0) % blocks
    out = jnp.zeros((rows, 128), F32)
    for b in range(blocks):
        out = jnp.where(part == b, taken[:, b * 128 : (b + 1) * 128], out)
    out_ref[...] = out.astype(BF16)


def pack(where, ids, x):
    rows = ids.shape[0]
    return pl.pallas_call(
        pack_kernel,
        name="pack",
        out_shape=jax.ShapeDtypeStruct((768, 128), BF16),
        grid_spec=pltpu.PrefetchScalarGridSpec(
            num_scalar_prefetch=1,
            grid=(1,),
            in_specs=[
                pl.BlockSpec((rows, ids.shape[1]), lambda i, s: (0, 0)),
                pl.BlockSpec((rows, 512), lambda i, s: (0, s[1])),
            ],
            out_specs=pl.BlockSpec((768, 128), lambda i, s: (0, 0)),
        ),
    )(where, ids, x)


def hidden_kernel(x_ref, w_ref, out_ref, wide_ref, rows_ref):
    for q in range(4):
        wide_ref[...] = x_ref[q].astype(F32)
        for b in range(4):
            rows_ref[:, (q * 4 + b) * 128 : (q * 4 + b + 1) * 128] = wide_ref[
                pl.ds(b, 192, stride=4), :
            ].astype(BF16)
    rows = rows_ref[...]
    for y in range(4):
        gate = jnp.dot(rows, w_ref[y, 0], preferred_element_type=F32)
        up = jnp.dot(rows, w_ref[y, 1], preferred_element_type=F32)
        hidden = (gate / (1.0 + jnp.exp(-gate)) * up).astype(BF16)
        for q in range(4):
            out_ref[q, :, y * 128 : (y + 1) * 128] = hidden


def hidden_of(x, w):
    return pl.pallas_call(
        hidden_kernel,
        name="hidden",
        out_shape=jax.ShapeDtypeStruct((4, 192, 512), BF16),
        in_specs=vmem(2),
        out_specs=vmem(1)[0],
        scratch_shapes=[pltpu.VMEM((768, 128), F32), pltpu.VMEM((192, 2048), BF16)],
    )(x, w)


def down_kernel(h_ref, w_ref, out_ref, rows_ref, wide_ref):
    for q in range(4):
        for y in range(4):
            rows_ref[:, (y * 4 + q) * 128 : (y * 4 + q + 1) * 128] = h_ref[
                q, :, y * 128 : (y + 1) * 128
            ]
    rows = rows_ref[...]
    for y in range(4):
        wide_ref[pl.ds(y, 192, stride=4), :] = jnp.dot(
            rows, w_ref[y], preferred_element_type=F32
        )
    out_ref[...] = wide_ref[...].astype(BF16)


def down_of(h, w):
    return pl.pallas_call(
        down_kernel,
        name="down",
        out_shape=jax.ShapeDtypeStruct((768, 128), BF16),
        in_specs=vmem(2),
        out_specs=vmem(1)[0],
        scratch_shapes=[pltpu.VMEM((192, 2048), BF16), pltpu.VMEM((768, 128), F32)],
    )(h, w)


def combine_kernel(where, ids_ref, weights_ref, back_ref, out_ref):
    slots, blocks = 6, 4
    cols = back_ref.shape[0]
    ids = ids_ref[...]
    code, experts = ordinals(ids)
    weight = jnp.zeros(experts.shape, F32)
    for k in range(ids.shape[1]):
        weight = weight + jnp.where(
            ids[:, k : k + 1] == experts, weights_ref[:, k : k + 1], 0.0
        )
    expert_of = (iota((128, cols), 1) // (slots * blocks) == iota((128, cols), 0)).astype(BF16)
    spread = jnp.dot(code, expert_of, preferred_element_type=F32)
    col = iota(spread.shape, 1)
    wanted = (col % (slots * blocks)) // blocks + (where[0] * slots + 1)
    here = spread == wanted.astype(F32)
    parts = []
    for _ in range(3):
        piece = weight.astype(BF16)
        weight = weight - piece.astype(F32)
        spread_piece = jnp.dot(piece, expert_of, preferred_element_type=F32)
        parts.append(jnp.where(here, spread_piece, 0.0).astype(BF16))
    back = back_ref[...]
    for b in range(blocks):
        total = jnp.zeros((ids.shape[0], 128), F32)
        for piece in reversed(parts):
            mine = jnp.where(col % blocks == b, piece, jnp.zeros_like(piece))
            total = total + jnp.dot(mine, back, preferred_element_type=F32)
        out_ref[b] = total


def combine(where, ids, weights, back):
    rows = ids.shape[0]
    return pl.pallas_call(
        combine_kernel,
        name="combine",
        out_shape=jax.ShapeDtypeStruct((4, rows, 128), F32),
        in_specs=[pl.BlockSpec(memory_space=pltpu.SMEM)] + vmem(3),
        out_specs=vmem(1)[0],
    )(where, ids, weights, back)


def wide_kernel(parts_ref, mix_ref, shared_ref, mixed_ref, sum_ref, rows_ref):
    for half, (w_ref, out_ref) in enumerate(((mix_ref, mixed_ref), (shared_ref, sum_ref))):
        for p in range(16):
            rows_ref[:, p * 128 : (p + 1) * 128] = parts_ref[p, half * 128 : half * 128 + 128, :]
        out_ref[...] = jnp.dot(rows_ref[...], w_ref[...], preferred_element_type=F32)


def wide_products(parts, mix_out, shared_down):
    return pl.pallas_call(
        wide_kernel,
        name="wide",
        out_shape=[jax.ShapeDtypeStruct((128, 128), F32)] * 2,
        in_specs=vmem(3),
        out_specs=vmem(2),
        scratch_shapes=[pltpu.VMEM((128, 2048), BF16)],
    )(parts, mix_out, shared_down)


def stats_kernel(partial_ref, shared_ref, mixed_ref, combined_ref, out_ref):
    combined = shared_ref[...] + (
        (partial_ref[0] + partial_ref[1]) + (partial_ref[2] + partial_ref[3])
    )
    combined_ref[...] = combined
    for place, values in ((0, mixed_ref[...]), (2, combined)):
        turned = values.T
        total = jnp.sum(turned, axis=0, keepdims=True)
        square = jnp.sum(turned * turned, axis=0, keepdims=True)
        for p in range(16):
            out_ref[p, place : place + 1, :] = total
            out_ref[p, place + 1 : place + 2, :] = square


def stats_of(partial, shared, mixed):
    return pl.pallas_call(
        stats_kernel,
        name="stats",
        out_shape=[
            jax.ShapeDtypeStruct((128, 128), F32),
            jax.ShapeDtypeStruct((16, 4, 128), F32),
        ],
        in_specs=vmem(3),
        out_specs=vmem(2),
    )(partial, shared, mixed)


def finish_kernel(stats_ref, mixed_ref, combined_ref, coef_ref, out_mixer_ref, out_experts_ref):
    totals = stats_ref[0]
    for p in range(1, 16):
        totals = totals + stats_ref[p]
    totals = totals / 2048.0
    for place, values_ref, out_ref in (
        (0, mixed_ref, out_mixer_ref),
        (2, combined_ref, out_experts_ref),
    ):
        average = totals[place : place + 1]
        spread = totals[place + 1 : place + 2] - average * average
        scale = lax.rsqrt(spread + 1e-05)
        average = jnp.broadcast_to(average, (128, 128)).T
        scale = jnp.broadcast_to(scale, (128, 128)).T
        scaled = (values_ref[...] - average) * scale
        out_ref[...] = (
            scaled * coef_ref[place : place + 1, :] + coef_ref[place + 1 : place + 2, :]
        ).astype(BF16)


def finish(stats, mixed, combined, coef):
    return pl.pallas_call(
        finish_kernel,
        name="finish",
        out_shape=[jax.ShapeDtypeStruct((128, 128), BF16)] * 2,
        in_specs=vmem(4),
        out_specs=vmem(2),
    )(stats, mixed, combined, coef)


def on_device(
    outer_gate,
    inner_gate,
    conv_value,
    conv_taps,
    mix_out,
    gain_mixer,
    bias_mixer,
    moe_input,
    route_ids,
    route_weights,
    expert_gate,
    expert_up,
    expert_down,
    shared_gate,
    shared_up,
    shared_down,
    gain_experts,
    bias_experts,
):
    token_rows, column_count = outer_gate.shape
    ep_count = lax.axis_size("ep")
    taps_count = conv_taps.shape[0]
    where = jnp.stack([lax.axis_index("y"), lax.axis_index("x")]).astype(jnp.int32)

    sent = pack(where, route_ids, moe_input)
    arrived = exchanged(sent.reshape(ep_count, 24, 128), "ep").reshape(768, 128)
    into_hidden = from_everyone(jnp.concatenate([expert_gate, expert_up]), "y").reshape(4, 2, 2048, 128)
    into_out = from_everyone(expert_down[0], "y")

    product = (inner_gate.astype(F32) * conv_value.astype(F32)).astype(BF16)
    border = shifted(product[token_rows - (taps_count - 1) :], "ep", 1)
    extended = jnp.concatenate([border, product], axis=0).astype(F32)
    seq_length = token_rows * ep_count // SEQS
    places = (
        lax.axis_index("ep") * token_rows + jnp.arange(token_rows, dtype=jnp.int32)
    ) % seq_length
    convolved = jnp.zeros((token_rows, column_count), F32)
    for offset in range(taps_count):
        delay_rows = taps_count - 1 - offset
        delayed = extended[offset : offset + token_rows]
        kept_mask = (places >= delay_rows).astype(F32)[:, None]
        convolved = convolved + conv_taps[offset].astype(F32)[None, :] * delayed * kept_mask
    weighted_in = (outer_gate.astype(F32) * convolved).astype(BF16)
    shared_gate_value = jnp.dot(moe_input, shared_gate, preferred_element_type=F32)
    shared_up_value = jnp.dot(moe_input, shared_up, preferred_element_type=F32)
    shared_hidden = (jax.nn.silu(shared_gate_value) * shared_up_value).astype(BF16)
    both = from_everyone(jnp.concatenate([weighted_in, shared_hidden]), TP)
    mixed, shared_sum = wide_products(both, mix_out, shared_down)

    rows = from_everyone(arrived, "x")
    hidden = exchanged(hidden_of(rows, into_hidden), "x")
    expert_out = down_of(hidden, into_out)
    back = exchanged(expert_out.reshape(ep_count, 24, 128), "ep").reshape(768, 128)
    partial = exchanged(combine(where, route_ids, route_weights, back), "y")
    combined, stats = stats_of(partial, shared_sum, mixed)
    stats = exchanged(stats, TP)
    coef = jnp.stack([gain_mixer, bias_mixer, gain_experts, bias_experts]).astype(F32)
    return tuple(finish(stats, mixed, combined, coef))


def solution(mesh):
    split = Mesh(mesh.devices.reshape(mesh.shape["ep"], 4, 4), ("ep", "y", "x"))
    placed = (
        P("ep", TP),
        P("ep", TP),
        P("ep", TP),
        P(None, TP),
        P(None, TP),
        P(TP),
        P(TP),
        P("ep", None),
        P("ep", None),
        P("ep", None),
        P("ep", None, TP),
        P("ep", None, TP),
        P("ep", None, TP),
        P(None, TP),
        P(None, TP),
        P(None, TP),
        P(TP),
        P(TP),
    )
    return jax.shard_map(
        on_device,
        mesh=split,
        in_specs=placed,
        out_specs=(P("ep", TP), P("ep", TP)),
        check_vma=False,
    )
```

time: 251 us -> 232 us (0.924)
  waiting for transfers between devices: 128 us -> 71.5 us
  blocking collectives: 52.5 us -> 86.6 us
  Pallas kernels: 0 us -> 21.2 us
  between operations: 14.5 us -> 0.88 us
  matrix products: 10.7 us -> 2.82 us
  starting transfers between devices: 30.9 us -> 36.4 us
    all_gather x2 -> x0, waiting for transfers between devices: 95.7 us -> none  [the longest x1 57.4 us: on_device(): piece = lax.all_gather(flat_hidden, TP, axis=1, tiled=True)]
    all_to_all x1 -> x2, blocking collectives: 35.4 us -> 86.6 us  [exchanged(): return lax.all_to_all(x, axis, split_axis=0, concat_axis=0, tiled=True)]
    all_to_all x4 -> x7, waiting for transfers between devices: 31.6 us -> 71.5 us  [exchanged(): return lax.all_to_all(x, axis, split_axis=0, concat_axis=0, tiled=True)]
    pallas_call x0 -> x7, Pallas kernels: none -> 21.2 us  [the longest x1 5.29 us: hidden_of(): pl.pallas_call(hidden_kernel, name='hidden', out_shape=jax.ShapeDtypeStru...]
    all_gather x1 -> x0, blocking collectives: 17.1 us -> none  [whole_of(): out = lax.all_gather(out, axes[number], axis=dim, tiled=True)]
    dot_general x7 -> x2, matrix products: 10.7 us -> 2.82 us  [the longest x1 1.49 us: on_device(): shared_up_value = jnp.dot(moe_input, shared_up, preferred_element_type=F32)]
    all_to_all x4 -> x7, starting transfers between devices: 29.3 us -> 35.1 us  [exchanged(): return lax.all_to_all(x, axis, split_axis=0, concat_axis=0, tiled=True)]
    scatter x1 -> x0, local copies, waits for them, and re-layouts: 3.04 us -> none  [on_device(): buffer_rows = buffer_rows.at[targets].set(sent_rows[sources])]
  transfers between devices with their start and end apart: 7 -> 8, of which waited for: 6 -> 7; matrix products, arithmetic and copies ran while one was open for 3% -> 2% of each run, Pallas kernels for 0% -> 6%
where the time goes in v1:
time: 232 us; the launch traced here: 231 us
  blocking collectives  86.6 us (37%)
  waiting for transfers between devices  71.5 us (31%)
  starting transfers between devices  36.4 us (16%)
  Pallas kernels  21.2 us (9%)
  local copies, waits for them, and re-layouts  8.86 us (4%)
  matrix products  2.82 us (1%)
  other arithmetic  2.7 us (1%)
    all_to_all x2, blocking collectives, exchanged(): return lax.all_to_all(x, axis, split_axis=0, concat_axis=0, tiled=True)  86.6 us
    all_to_all x7, waiting for transfers between devices, exchanged(): return lax.all_to_all(x, axis, split_axis=0, concat_axis=0, tiled=True)  71.5 us
    all_to_all x7, starting transfers between devices, exchanged(): return lax.all_to_all(x, axis, split_axis=0, concat_axis=0, tiled=True)  35.1 us
    pallas_call x1, Pallas kernels, hidden_of(): pl.pallas_call(hidden_kernel, name='hidden', out_shape=jax.ShapeDtypeStru...  5.29 us
  transfers between devices with their start and end apart: 8, of which 7 were waited for; matrix products, arithmetic and copies ran while one was open for 2% of the time, Pallas kernels for 6%

profile of v1, /device:TPU:2, one launch (start us, length us, event | category | flops | bytes accessed | tf_op | source)
XLA Modules:
  0.0 230.9 jit_solution(9045195766360663810)
XLA Ops:
  2.7 3.2 %pack.1 = bf16[768,128]{1,0:T(8,128)(2,1)} custom-call(s32[2]{0:T(128)} %pad_add_fusion.where, s32[128,4]{1,0:T(8,128)} %copy.21.ids_ref, bf16[128,2048]{1,0:T(8,128)(2,1)} %x_ref.1), custom_call_target="tpu_custom_call" | custom-call | tf_op jit(solution)/shard_map/pack/pallas_call | solution.py:69
  6.0 35.5 %all_to_all.45 = bf16[32,24,128]{2,1,0:T(8,128)(2,1)S(1)} all-to-all(bf16[32,24,128]{2,1,0:T(8,128)(2,1)} %bitcast.26), channel_id=1, replica_groups=mesh['ep'=32,'y'=4,'x'=4] {'ep'}, dimensions={0} | all-to-all | bytes 393216 | tf_op jit(solution)/shard_map/all_to_all | solution.py:22
  42.4 4.8 %all-to-all-start.1 = ((bf16[4,768,128]{2,1,0:T(8,128)(2,1)}), bf16[4,768,128]{2,1,0:T(8,128)(2,1)S(1)}, u32[]{:S(2)}, u32[]{:S(2)}) async-start(bf16[4,768,128]{2,1,0:T(8,128)(2,1)} %broadcast_in_dim.8), calls=%async_computation.1 | async-start | bytes 1572864 | tf_op jit(solution)/shard_map/all_to_all | solution.py:22
  48.6 8.8 %all-to-all-done.1.x_ref = bf16[4,768,128]{2,1,0:T(8,128)(2,1)S(1)} async-done(((bf16[4,768,128]{2,1,0:T(8,128)(2,1)}), bf16[4,768,128]{2,1,0:T(8,128)(2,1)S(1)}, u32[]{:S(2)}, u32[]{:S(2)}) %all-to-all-start.1) | async-done | bytes 786464 | tf_op jit(solution)/shard_map/all_to_all | solution.py:22
  57.9 51.1 %all_to_all.46.w_ref = bf16[4,2,2048,128]{3,2,1,0:T(8,128)(2,1)} all-to-all(bf16[4,2,2048,128]{3,2,1,0:T(8,128)(2,1)S(1)} %broadcast_in_dim.9), channel_id=1, replica_groups=mesh['ep'=32,'y'=4,'x'=4] {'y'}, dimensions={0} | all-to-all | bytes 8388608 | tf_op jit(solution)/shard_map/all_to_all | solution.py:22
  109.0 1.7 broadcast_in_dim.20
  110.6 3.6 %all-to-all-start.4 = ((bf16[4,2048,128]{2,1,0:T(8,128)(2,1)}), bf16[4,2048,128]{2,1,0:T(8,128)(2,1)S(1)}, u32[]{:S(2)}, u32[]{:S(2)}) async-start(bf16[4,2048,128]{2,1,0:T(8,128)(2,1)} %broadcast_in_dim.20), calls=%async_computation.4 | async-start | bytes 4194304 | tf_op jit(solution)/shard_map/all_to_all | solution.py:22
  115.6 5.3 %hidden.1 = bf16[4,192,512]{2,1,0:T(8,128)(2,1)} custom-call(bf16[4,768,128]{2,1,0:T(8,128)(2,1)} %copy-done.4, bf16[4,2,2048,128]{3,2,1,0:T(8,128)(2,1)} %all_to_all.46.w_ref), custom_call_target="tpu_custom_call" | custom-call | tf_op jit(solution)/shard_map/hidden/pallas_call | solution.py:102
  120.9 16.6 %all-to-all-done.4.w_ref = bf16[4,2048,128]{2,1,0:T(8,128)(2,1)S(1)} async-done(((bf16[4,2048,128]{2,1,0:T(8,128)(2,1)}), bf16[4,2048,128]{2,1,0:T(8,128)(2,1)S(1)}, u32[]{:S(2)}, u32[]{:S(2)}) %all-to-all-start.4) | async-done | bytes 2097184 | tf_op jit(solution)/shard_map/all_to_all | solution.py:22
  137.5 4.9 %all-to-all-start.3 = ((bf16[4,192,512]{2,1,0:T(8,128)(2,1)}), bf16[4,192,512]{2,1,0:T(8,128)(2,1)S(1)}, u32[]{:S(2)}, u32[]{:S(2)}) async-start(bf16[4,192,512]{2,1,0:T(8,128)(2,1)} %hidden.1), calls=%async_computation.3 | async-start | bytes 1572864 | tf_op jit(solution)/shard_map/all_to_all | solution.py:22
  145.3 5.2 %all-to-all-done.3.h_ref = bf16[4,192,512]{2,1,0:T(8,128)(2,1)S(1)} async-done(((bf16[4,192,512]{2,1,0:T(8,128)(2,1)}), bf16[4,192,512]{2,1,0:T(8,128)(2,1)S(1)}, u32[]{:S(2)}, u32[]{:S(2)}) %all-to-all-start.3) | async-done | bytes 786464 | tf_op jit(solution)/shard_map/all_to_all | solution.py:22
  151.3 3.5 %down.1 = bf16[768,128]{1,0:T(8,128)(2,1)} custom-call(bf16[4,192,512]{2,1,0:T(8,128)(2,1)} %copy-done.3, bf16[4,2048,128]{2,1,0:T(8,128)(2,1)} %copy-done.1), custom_call_target="tpu_custom_call" | custom-call | tf_op jit(solution)/shard_map/down/pallas_call | solution.py:127
  154.9 8.3 %all-to-all-start.5 = ((bf16[32,24,128]{2,1,0:T(8,128)(2,1)}), bf16[32,24,128]{2,1,0:T(8,128)(2,1)S(1)}, u32[]{:S(2)}, u32[]{:S(2)}) async-start(bf16[32,24,128]{2,1,0:T(8,128)(2,1)} %bitcast.24), calls=%async_computation.5 | async-start | bytes 393216 | tf_op jit(solution)/shard_map/all_to_all | solution.py:22
  163.5 19.8 %all-to-all-done.5 = bf16[32,24,128]{2,1,0:T(8,128)(2,1)S(1)} async-done(((bf16[32,24,128]{2,1,0:T(8,128)(2,1)}), bf16[32,24,128]{2,1,0:T(8,128)(2,1)S(1)}, u32[]{:S(2)}, u32[]{:S(2)}) %all-to-all-start.5) | async-done | bytes 196640 | tf_op jit(solution)/shard_map/all_to_all | solution.py:22
  184.4 4.9 %all-to-all-start.7 = ((bf16[16,256,128]{2,1,0:T(8,128)(2,1)}), bf16[16,256,128]{2,1,0:T(8,128)(2,1)S(1)}, u32[]{:S(2)}, u32[]{:S(2)}) async-start(bf16[16,256,128]{2,1,0:T(8,128)(2,1)} %broadcast_in_dim.21), calls=%async_computation.7 | async-start | bytes 2097152 | tf_op jit(solution)/shard_map/all_to_all | solution.py:22
  190.1 3.0 %combine.1 = f32[4,128,128]{2,1,0:T(8,128)} custom-call(s32[2]{0:T(128)} %pad_add_fusion.where, s32[128,4]{1,0:T(8,128)} %copy.21.ids_ref, f32[128,4]{1,0:T(8,128)} %copy.22.weights_ref, bf16[768,128]{1,0:T(8,128)(2,1)} %bitcast.25), custom_call_target="tpu_custom_call" | custom-call | tf_op jit(solution)/shard_map/combine/pallas_call | solution.py:169
  193.1 11.6 %all-to-all-done.7.parts_ref = bf16[16,256,128]{2,1,0:T(8,128)(2,1)S(1)} async-done(((bf16[16,256,128]{2,1,0:T(8,128)(2,1)}), bf16[16,256,128]{2,1,0:T(8,128)(2,1)S(1)}, u32[]{:S(2)}, u32[]{:S(2)}) %all-to-all-start.7) | async-done | bytes 1048608 | tf_op jit(solution)/shard_map/all_to_all | solution.py:22
  204.7 3.4 %all-to-all-start.6 = ((f32[4,128,128]{2,1,0:T(8,128)}), f32[4,128,128]{2,1,0:T(8,128)S(1)}, u32[]{:S(2)}, u32[]{:S(2)}) async-start(f32[4,128,128]{2,1,0:T(8,128)} %combine.1), calls=%async_computation.6 | async-start | bytes 524288 | tf_op jit(solution)/shard_map/all_to_all | solution.py:22
  208.1 2.7 %wide.1 = (f32[128,128]{1,0:T(8,128)}, f32[128,128]{1,0:T(8,128)}) custom-call(bf16[16,256,128]{2,1,0:T(8,128)(2,1)} %copy-done.2, bf16[2048,128]{1,0:T(8,128)(2,1)} %mix_ref.1, bf16[2048,128]{1,0:T(8,128)(2,1)} %shared_ref.1), custom_call_target="tpu_custom_call" | custom-call | tf_op jit(solution)/shard_map/wide/pallas_call | solution.py:186
  210.8 3.9 %all-to-all-done.6.partial_ref = f32[4,128,128]{2,1,0:T(8,128)S(1)} async-done(((f32[4,128,128]{2,1,0:T(8,128)}), f32[4,128,128]{2,1,0:T(8,128)S(1)}, u32[]{:S(2)}, u32[]{:S(2)}) %all-to-all-start.6) | async-done | bytes 262176 | tf_op jit(solution)/shard_map/all_to_all | solution.py:22
  215.5 1.7 stats.1
  217.2 5.2 %all-to-all-start.8 = ((f32[16,4,128]{2,1,0:T(4,128)}), f32[16,4,128]{2,1,0:T(4,128)S(1)}, u32[]{:S(2)}, u32[]{:S(2)}) async-start(f32[16,4,128]{2,1,0:T(4,128)} %get-tuple-element.8), calls=%async_computation.8 | async-start | bytes 65536 | tf_op jit(solution)/shard_map/all_to_all | solution.py:22
  223.0 5.7 %all-to-all-done.8.stats_ref = f32[16,4,128]{2,1,0:T(4,128)S(1)} async-done(((f32[16,4,128]{2,1,0:T(4,128)}), f32[16,4,128]{2,1,0:T(4,128)S(1)}, u32[]{:S(2)}, u32[]{:S(2)}) %all-to-all-start.8) | async-done | bytes 32800 | tf_op jit(solution)/shard_map/all_to_all | solution.py:22
  229.3 1.7 finish.1
  (56 shorter events, 14.0 us)
Async XLA Ops:
  0.6 141.8 %copy-start = (bf16[2048,128]{1,0:T(8,128)(2,1)S(1)}, bf16[2048,128]{1,0:T(8,128)(2,1)}, u32[]{:S(2)}) copy-start(bf16[2048,128]{1,0:T(8,128)(2,1)} %param.31) | copy-start | bytes 1572868
  42.4 14.9 %all-to-all-start.1 = ((bf16[4,768,128]{2,1,0:T(8,128)(2,1)}), bf16[4,768,128]{2,1,0:T(8,128)(2,1)S(1)}, u32[]{:S(2)}, u32[]{:S(2)}) async-start(bf16[4,768,128]{2,1,0:T(8,128)(2,1)} %broadcast_in_dim.8), calls=%async_computation.1 | async-start | bytes 1572864 | tf_op jit(solution)/shard_map/all_to_all | solution.py:22
  57.3 51.7 %copy-start.4 = (bf16[4,768,128]{2,1,0:T(8,128)(2,1)}, bf16[4,768,128]{2,1,0:T(8,128)(2,1)S(1)}, u32[]{:S(2)}) copy-start(bf16[4,768,128]{2,1,0:T(8,128)(2,1)S(1)} %all-to-all-done.1.x_ref) | copy-start | bytes 2359300
  57.9 51.1 %copy-start.7 = (bf16[1,2048,128]{2,1,0:T(8,128)(2,1)S(1)}, bf16[1,2048,128]{2,1,0:T(8,128)(2,1)}, u32[]{:S(2)}) copy-start(bf16[1,2048,128]{2,1,0:T(8,128)(2,1)} %param.30) | copy-start | bytes 1572868
  109.0 5.3 %copy-start.9 = (bf16[128,128]{1,0:T(8,128)(2,1)S(1)}, bf16[128,128]{1,0:T(8,128)(2,1)}, u32[]{:S(2)}) copy-start(bf16[128,128]{1,0:T(8,128)(2,1)} %param.20) | copy-start | bytes 98308
  109.0 5.3 %copy-start.10 = (bf16[128,128]{1,0:T(8,128)(2,1)S(1)}, bf16[128,128]{1,0:T(8,128)(2,1)}, u32[]{:S(2)}) copy-start(bf16[128,128]{1,0:T(8,128)(2,1)} %param.19) | copy-start | bytes 98308
  110.6 26.8 %all-to-all-start.4 = ((bf16[4,2048,128]{2,1,0:T(8,128)(2,1)}), bf16[4,2048,128]{2,1,0:T(8,128)(2,1)S(1)}, u32[]{:S(2)}, u32[]{:S(2)}) async-start(bf16[4,2048,128]{2,1,0:T(8,128)(2,1)} %broadcast_in_dim.20), calls=%async_computation.4 | async-start | bytes 4194304 | tf_op jit(solution)/shard_map/all_to_all | solution.py:22
  114.3 49.0 %collective-permute-start = (bf16[2,128]{1,0:T(2,128)(2,1)S(1)}, bf16[2,128]{1,0:T(2,128)(2,1)S(1)}, u32[]{:S(2)}, u32[]{:S(2)}) collective-permute-start(bf16[2,128]{1,0:T(2,128)(2,1)S(1)} %slice.28), channel_id=1, source_target_pairs={{0,16},{16,32},{32,48},{48,64},{64,80},{80,96},{96,112},{112,128},... | collective-permute-start | bytes 1544 | tf_op jit(solution)/shard_map/ppermute | solution.py:18
  120.9 42.3 %copy-start.12 = (bf16[3,128]{1,0:T(4,128)(2,1)S(1)}, bf16[3,128]{1,0:T(4,128)(2,1)}, u32[]{:S(2)}) copy-start(bf16[3,128]{1,0:T(4,128)(2,1)} %param.21) | copy-start | bytes 2308
  120.9 42.4 %copy-start.11 = (bf16[128,128]{1,0:T(8,128)(2,1)S(1)}, bf16[128,128]{1,0:T(8,128)(2,1)}, u32[]{:S(2)}) copy-start(bf16[128,128]{1,0:T(8,128)(2,1)} %param.18) | copy-start | bytes 98308
  137.5 13.0 %copy-start.1 = (bf16[4,2048,128]{2,1,0:T(8,128)(2,1)}, bf16[4,2048,128]{2,1,0:T(8,128)(2,1)S(1)}, u32[]{:S(2)}) copy-start(bf16[4,2048,128]{2,1,0:T(8,128)(2,1)S(1)} %all-to-all-done.4.w_ref) | copy-start | bytes 6291460
  137.5 13.0 %all-to-all-start.3 = ((bf16[4,192,512]{2,1,0:T(8,128)(2,1)}), bf16[4,192,512]{2,1,0:T(8,128)(2,1)S(1)}, u32[]{:S(2)}, u32[]{:S(2)}) async-start(bf16[4,192,512]{2,1,0:T(8,128)(2,1)} %hidden.1), calls=%async_computation.3 | async-start | bytes 1572864 | tf_op jit(solution)/shard_map/all_to_all | solution.py:22
  143.8 45.5 %copy-start.13 = (f32[128,4]{0,1:T(4,128)S(1)}, f32[128,4]{0,1:T(4,128)}, u32[]{:S(2)}) copy-start(f32[128,4]{0,1:T(4,128)} %param.27) | copy-start | bytes 6148
  150.5 0.9 copy-start.3
  154.9 67.4 %copy-start.14 = (bf16[128]{0:T(256)(128)(2,1)S(1)}, bf16[128]{0:T(256)(128)(2,1)}, u32[]{:S(2)}) copy-start(bf16[128]{0:T(256)(128)(2,1)} %param.35) | copy-start | bytes 772
  154.9 67.4 %copy-start.15 = (bf16[128]{0:T(256)(128)(2,1)S(1)}, bf16[128]{0:T(256)(128)(2,1)}, u32[]{:S(2)}) copy-start(bf16[128]{0:T(256)(128)(2,1)} %param.34) | copy-start | bytes 772
  154.9 67.5 %copy-start.16 = (bf16[128]{0:T(256)(128)(2,1)S(1)}, bf16[128]{0:T(256)(128)(2,1)}, u32[]{:S(2)}) copy-start(bf16[128]{0:T(256)(128)(2,1)} %param.24) | copy-start | bytes 772
  154.9 67.5 %copy-start.17 = (bf16[128]{0:T(256)(128)(2,1)S(1)}, bf16[128]{0:T(256)(128)(2,1)}, u32[]{:S(2)}) copy-start(bf16[128]{0:T(256)(128)(2,1)} %param.23) | copy-start | bytes 772
  154.9 28.3 %all-to-all-start.5 = ((bf16[32,24,128]{2,1,0:T(8,128)(2,1)}), bf16[32,24,128]{2,1,0:T(8,128)(2,1)S(1)}, u32[]{:S(2)}, u32[]{:S(2)}) async-start(bf16[32,24,128]{2,1,0:T(8,128)(2,1)} %bitcast.24), calls=%async_computation.5 | async-start | bytes 393216 | tf_op jit(solution)/shard_map/all_to_all | solution.py:22
  183.2 6.8 %copy-start.6 = (bf16[32,24,128]{2,1,0:T(8,128)(2,1)}, bf16[32,24,128]{2,1,0:T(8,128)(2,1)S(1)}, u32[]{:S(2)}) copy-start(bf16[32,24,128]{2,1,0:T(8,128)(2,1)S(1)} %all-to-all-done.5) | copy-start | bytes 589828
  184.4 20.3 %all-to-all-start.7 = ((bf16[16,256,128]{2,1,0:T(8,128)(2,1)}), bf16[16,256,128]{2,1,0:T(8,128)(2,1)S(1)}, u32[]{:S(2)}, u32[]{:S(2)}) async-start(bf16[16,256,128]{2,1,0:T(8,128)(2,1)} %broadcast_in_dim.21), calls=%async_computation.7 | async-start | bytes 2097152 | tf_op jit(solution)/shard_map/all_to_all | solution.py:22
  204.7 3.4 %copy-start.2 = (bf16[16,256,128]{2,1,0:T(8,128)(2,1)}, bf16[16,256,128]{2,1,0:T(8,128)(2,1)S(1)}, u32[]{:S(2)}) copy-start(bf16[16,256,128]{2,1,0:T(8,128)(2,1)S(1)} %all-to-all-done.7.parts_ref) | copy-start | bytes 3145732
  204.7 10.1 %all-to-all-start.6 = ((f32[4,128,128]{2,1,0:T(8,128)}), f32[4,128,128]{2,1,0:T(8,128)S(1)}, u32[]{:S(2)}, u32[]{:S(2)}) async-start(f32[4,128,128]{2,1,0:T(8,128)} %combine.1), calls=%async_computation.6 | async-start | bytes 524288 | tf_op jit(solution)/shard_map/all_to_all | solution.py:22
  217.2 11.5 %all-to-all-start.8 = ((f32[16,4,128]{2,1,0:T(4,128)}), f32[16,4,128]{2,1,0:T(4,128)S(1)}, u32[]{:S(2)}, u32[]{:S(2)}) async-start(f32[16,4,128]{2,1,0:T(4,128)} %get-tuple-element.8), calls=%async_computation.8 | async-start | bytes 65536 | tf_op jit(solution)/shard_map/all_to_all | solution.py:22
  (2 other events, 1.3 us)
